TPU v7x, 32 devices: a whole 2x2x4 slice. The times are simulated.
32 devices in a mesh: ep: 8 (over z, y), tp: 4 (over x, core).
Axes of the slice: x: 2, y: 2, z: 4, core: 2. Of those that a mesh axis runs over, the one named last changes fastest.
Arguments:
- conv_value: bfloat16 [12288, 2048], P(('ep', 'tp')), may hold values from -6 to 6
- conv_gate: bfloat16 [12288, 2048], P(('ep', 'tp')), may hold values from -6 to 6
- conv_taps: float32 [31, 2048], replicated, may hold values from -1 to 1
- conv_gain: float32 [2048], replicated, may hold values from 0.1 to 1.9
- conv_bias: float32 [2048], replicated, may hold values from -3 to 3
- conv_projection: bfloat16 [2048, 4096], P(None, 'tp'), may hold values from -0.125 to 0.125
- expert_input: bfloat16 [4096, 4096], P('ep'), may hold values from -6 to 6
- expert_gain: float32 [4096], replicated, may hold values from 0.1 to 1.9
- route_experts: int32 [4096, 2], P('ep'), may hold values from 0 to 31, all different within a row; in each aligned block of 128 rows (0 to 127, 128 to 255, ...) at most 16 rows name the same one
- group_gate: float32 [4096], P('ep'), may hold values from 0.3 to 1
- expert_gate: float32 [4096, 2], P('ep'), may hold values from 0.1 to 1
- gate_weight: bfloat16 [32, 4096, 1024], P('ep', None, 'tp'), may hold values from -0.09375 to 0.09375
- up_weight: bfloat16 [32, 4096, 1024], P('ep', None, 'tp'), may hold values from -0.09375 to 0.09375
- down_weight: bfloat16 [32, 1024, 4096], P('ep', None, 'tp'), may hold values from -0.1875 to 0.1875
Outputs:
- conv_out: bfloat16 [12288, 4096], P('ep', 'tp')
- expert_out: bfloat16 [4096, 4096], P('ep', 'tp')
Inputs may be any that keep to these rules, and one draw needn't show every extreme that they name: `route_experts`: each row names 2 different experts; in each aligned block of 128 rows no expert is named more than 16 times, and in some blocks one expert is named exactly 16 times.
All inputs are finite; a program needn't handle non-finite values.
Results may differ from a plain program's by a relative error of at most 0.0071.
Values may be sent and summed in bfloat16 or wider, within the bound.
A program may use at most 128 MiB of HBM per device.

v0:
```python
import jax
import jax.numpy as jnp
from jax import lax
from jax.sharding import PartitionSpec as P

EXPERTS = 32
TOP = 2
MOE_DEV = 128
CAP = 16
epsilon = 1e-06


def passed_along(value, axis, steps):
    count = lax.axis_size(axis)
    leading, last = (max(0, -steps), min(count, count - steps))
    return lax.ppermute(value, axis, [(source, source + steps) for source in range(leading, last)])


def root_mean_norm(values, gain):
    widened = values.astype(jnp.float32)
    inverse_rms = lax.rsqrt(jnp.mean(widened * widened, axis=-1, keepdims=True) + epsilon)
    return (widened * inverse_rms * gain).astype(jnp.bfloat16)


def slot_positions(route_block):
    picked_experts = route_block.reshape(route_block.shape[0] // MOE_DEV, MOE_DEV * TOP)
    onehot = (
        picked_experts[:, :, None] == jnp.arange(EXPERTS, dtype=jnp.int32)[None, None, :]
    ).astype(jnp.int32)
    before = jnp.cumsum(onehot, axis=1) - onehot
    return (picked_experts, jnp.sum(before * onehot, axis=2))


def one_table(slot_index, token_index):
    return jnp.full((EXPERTS * CAP,), -1, jnp.int32).at[slot_index].set(token_index)


def take_rows(normed, source):
    return jnp.take(normed, jnp.maximum(source, 0), axis=0)


def fill_slots(normed, picked_experts, positions):
    slot_index = picked_experts * CAP + positions
    token_index = jnp.broadcast_to(
        jnp.arange(MOE_DEV * TOP, dtype=jnp.int32) // TOP, slot_index.shape
    )
    source = jax.vmap(one_table)(slot_index, token_index)
    taken_rows = jax.vmap(take_rows)(normed, source)
    taken_rows = jnp.where((source >= 0)[:, :, None], taken_rows, jnp.zeros_like(taken_rows))
    return taken_rows.reshape(normed.shape[0], EXPERTS, CAP, normed.shape[2])


def on_device(
    conv_value,
    conv_gate,
    conv_taps,
    conv_gain,
    conv_bias,
    conv_projection,
    expert_input,
    expert_gain,
    route_experts,
    group_gate,
    expert_gate,
    gate_weight,
    up_weight,
    down_weight,
):
    gated_rows = (
        conv_value.astype(jnp.float32) * jax.nn.sigmoid(conv_gate.astype(jnp.float32))
    ).astype(jnp.bfloat16)
    reach_back = conv_taps.shape[0] - 1
    length = gated_rows.shape[0]
    earlier = passed_along(gated_rows[length - reach_back :], ("ep", "tp"), 1)
    extended = jnp.concatenate([earlier, gated_rows], axis=0)
    mixed_conv = jnp.zeros(gated_rows.shape, jnp.float32)
    for lag_step in range(reach_back + 1):
        window = lax.slice_in_dim(
            extended, reach_back - lag_step, reach_back - lag_step + length, axis=0
        )
        mixed_conv = mixed_conv + conv_taps[lag_step] * window.astype(jnp.float32)
    center = mixed_conv - jnp.mean(mixed_conv, axis=-1, keepdims=True)
    spread = jnp.mean(center * center, axis=-1, keepdims=True)
    activated = jax.nn.silu(center * lax.rsqrt(spread + epsilon) * conv_gain + conv_bias).astype(
        jnp.bfloat16
    )
    conv_out = jnp.dot(
        lax.all_gather(activated, "tp", axis=0, tiled=True),
        conv_projection,
        preferred_element_type=jnp.float32,
    ).astype(jnp.bfloat16)
    quarters = lax.axis_size("tp")
    own_quarter = lax.axis_index("tp")
    picked_experts, positions = slot_positions(route_experts)
    own_rows = lax.dynamic_slice_in_dim(expert_input, own_quarter * MOE_DEV, MOE_DEV, 0)
    normed = root_mean_norm(own_rows, expert_gain)[None]
    own_experts = lax.dynamic_slice_in_dim(picked_experts, own_quarter, 1, 0)
    own_positions = lax.dynamic_slice_in_dim(positions, own_quarter, 1, 0)
    outgoing = fill_slots(normed, own_experts, own_positions)
    arrived = lax.all_to_all(outgoing, "ep", split_axis=1, concat_axis=2, tiled=True)
    hidden_arrived = lax.all_gather(arrived, "tp", axis=0, tiled=True)
    gate_part = jnp.einsum(
        "qecd,edh->qech", hidden_arrived, gate_weight, preferred_element_type=jnp.float32
    )
    up_part = jnp.einsum(
        "qecd,edh->qech", hidden_arrived, up_weight, preferred_element_type=jnp.float32
    )
    hidden = (jax.nn.silu(gate_part) * up_part).astype(jnp.bfloat16)
    summed = jnp.einsum(
        "qech,ehd->qecd",
        lax.all_gather(hidden, "tp", axis=3, tiled=True),
        down_weight,
        preferred_element_type=jnp.float32,
    )
    returned = lax.all_to_all(
        summed.astype(jnp.bfloat16), "ep", split_axis=2, concat_axis=1, tiled=True
    )
    result_table = returned.reshape(quarters * EXPERTS * CAP, returned.shape[3])
    plane_index = jnp.arange(quarters, dtype=jnp.int32)[:, None]
    slot_index = (plane_index * EXPERTS + picked_experts) * CAP + positions
    picked = jnp.take(result_table, slot_index.reshape(-1), axis=0).reshape(
        -1, TOP, returned.shape[3]
    )
    route_share = group_gate[:, None] * expert_gate / jnp.sum(expert_gate, axis=1, keepdims=True)
    expert_out = jnp.sum(picked.astype(jnp.float32) * route_share[:, :, None], axis=1).astype(
        jnp.bfloat16
    )
    return (conv_out, expert_out)


def solution(mesh):
    return jax.shard_map(
        on_device,
        mesh=mesh,
        in_specs=(
            P(("ep", "tp"), None),
            P(("ep", "tp"), None),
            P(),
            P(),
            P(),
            P(None, "tp"),
            P("ep", None),
            P(),
            P("ep", None),
            P("ep"),
            P("ep", None),
            P("ep", None, "tp"),
            P("ep", None, "tp"),
            P("ep", None, "tp"),
        ),
        out_specs=(P("ep", "tp"), P("ep", "tp")),
        check_vma=False,
    )
```

profile of v0, /device:TPU:0, one launch (start us, length us, event | category | flops | bytes accessed | tf_op | source)
XLA Modules:
  0.0 455.0 jit_solution(18274439870365131275)
XLA Ops:
  7.2 0.0 all-gather.6.cloned.1.call-start
  7.2 0.8 copy.45
  8.0 0.2 eq.29
  8.2 0.2 eq.25
  8.4 2.3 reduce-window.6
  10.8 0.1 slice.321
  10.9 0.1 copy.47
  11.0 0.1 fusion.49
  11.2 1.4 scatter_custom_fusion
  12.6 1.5 fusion.8
  14.2 0.1 broadcast_in_dim.62
  14.3 0.1 broadcast_in_dim.64
  14.3 1.6 fusion.46
  15.9 17.4 %gather_fusion.1 = bf16[512,4096]{1,0:T(8,128)(2,1)} fusion(bf16[1,128,4096]{2,1,0:T(8,128)(2,1)S(1)} %fusion.46, s32[512]{0:T(512)S(1)} %bitcast.132), kind=kCustom, calls=%fused_computation.1 | custom fusion | bytes 8392704 | tf_op jit(solution)/shard_map/vmap(jit(_take))/gather | solution.py:39
  33.4 2.6 select_select_fusion
  35.9 100.3 %all_to_all.33 = bf16[1,32,16,4096]{3,2,0,1:T(8,128)(2,1)S(1)} all-to-all(bf16[1,32,16,4096]{3,2,0,1:T(8,128)(2,1)S(1)} %select_select_fusion), channel_id=1, replica_groups=mesh['ep'=8,'tp'=4] {'ep'}, dimensions={1} | all-to-all | bytes 8388608 | tf_op jit(solution)/shard_map/all_to_all | solution.py:100
  136.2 2.2 copy.53
  138.4 0.0 all-gather.6.cloned.1.call-update
  138.4 0.2 all-gather.8.cloned.1.call-start
  138.7 104.8 %all-gather.6.cloned.1.call-done = bf16[4,4,128,4096]{3,2,0,1:T(8,128)(2,1)} async-done(((bf16[1,4,128,4096]{3,2,0,1:T(8,128)(2,1)}), bf16[4,4,128,4096]{3,2,0,1:T(8,128)(2,1)}) %all-gather.6.cloned.1.call-update) | async-done | bytes 16777232 | tf_op jit(solution)/shard_map/all_gather | solution.py:101
  243.5 14.0 %fusion.2 = f32[4,4,128,256]{3,2,1,0:T(8,128)} fusion(bf16[4,4,128,4096]{3,2,0,1:T(8,128)(2,1)} %all-gather.6.cloned.1.call-done, bf16[4,4096,256]{2,1,0:T(8,128)(2,1)} %param.26), kind=kOutput, calls=%fused_computation.34 | convolution fusion | flops 4294967296 | bytes 27262976 | tf_op jit(solution)/shard_map/qecd,edh->qech/dot_general | solution.py:105
  257.5 14.6 %fusion.11 = bf16[4,4,128,256]{3,2,0,1:T(8,128)(2,1)} fusion(f32[4,4,128,256]{3,2,1,0:T(8,128)} %fusion.2, bf16[4,4,128,4096]{3,2,0,1:T(8,128)(2,1)} %all-gather.6.cloned.1.call-done, bf16[4,4096,256]{2,1,0:T(8,128)(2,1)} %param.25), kind=kOutput, calls=%fused_computation.53 | convolution fusion | flops 4298113024 | bytes 28311552 | tf_op jit(solution)/shard_map/qecd,edh->qech/dot_general | solution.py:102
  272.0 0.0 copy-start.1
  272.0 0.0 all-gather.8.cloned.1.call-update
  272.1 0.0 all-gather.4.cloned.1.call-start
  272.1 0.0 copy-done
  272.1 2.3 multiply_convert_fusion.1
  274.5 2.4 collective-permute-start
  276.9 0.0 copy-done.1
  276.9 0.1 fusion.60
  277.0 0.1 fusion.61
  277.1 0.5 collective-permute-done
  277.6 0.0 copy-start.4
  277.6 0.0 copy-start.5
  277.6 14.3 %fusion.59 = (f32[384]{0:T(512)S(1)}, f32[384,2048]{1,0:T(8,128)S(1)}) fusion(bf16[384,2048]{1,0:T(8,128)(2,1)S(1)} %multiply_convert_fusion.1, bf16[30,2048]{1,0:T(8,128)(2,1)S(1)} %collective-permute-done, f32[2048]{0:T(1024)S(1)} %bitcast.166, f32[2048]{0:T(1024)S(1)} %bitcast.167, f32[2048]{0:T(1024)S(1)} %bitcast.138, f32[2048]{0:T(1024)S(1)} %bitcast.139, ...), kind=kLoop, calls=%fused_computation.136 | loop fusion | flops 143916672 | bytes 5096960 | tf_op jit(solution)/shard_map/reduce_sum | solution.py:82
  292.0 0.5 multiply_reduce_fusion.1
  292.4 0.0 copy-done.4
  292.4 0.0 copy-done.5
  292.4 2.4 multiply_convert_fusion
  294.8 0.0 all-gather.4.cloned.1.call-update
  294.8 12.4 %all-gather.8.cloned.1.call-done = bf16[4,4,128,1024]{3,2,0,1:T(8,128)(2,1)} async-done(((bf16[4,4,128,256]{3,2,0,1:T(8,128)(2,1)}), bf16[4,4,128,1024]{3,2,0,1:T(8,128)(2,1)}) %all-gather.8.cloned.1.call-update) | async-done | bytes 4194320 | tf_op jit(solution)/shard_map/all_gather | solution.py:111
  307.2 9.2 %convert_bitcast_fusion = bf16[4,4,128,1024]{3,2,0,1:T(8,128)(2,1)S(1)} fusion(bf16[4,4,128,1024]{3,2,0,1:T(8,128)(2,1)} %all-gather.8.cloned.1.call-done, bf16[4,1024,1024]{2,1,0:T(8,128)(2,1)} %param.27), kind=kOutput, calls=%fused_computation.39 | convolution fusion | flops 4297064448 | bytes 16777216 | tf_op jit(solution)/shard_map/qech,ehd->qecd/dot_general | solution.py:109
  316.4 5.3 %copy.54 = bf16[4,4,128,1024]{3,0,1,2:T(4,128)(2,1)} copy(bf16[4,4,128,1024]{3,2,0,1:T(8,128)(2,1)S(1)} %convert_bitcast_fusion) | data formatting | bytes 8388608 | tf_op jit(solution)/shard_map/convert_element_type | solution.py:116
  321.7 0.0 copy-start.2
  321.7 0.0 copy-start.3
  321.7 0.0 copy-start.6
  321.7 5.6 %all-to-all-start.1 = ((bf16[4,4,128,1024]{3,0,1,2:T(4,128)(2,1)}), bf16[4,4,128,1024]{3,0,1,2:T(4,128)(2,1)}, u32[]{:S(2)}, u32[]{:S(2)}) async-start(bf16[4,4,128,1024]{3,0,1,2:T(4,128)(2,1)} %copy.54), calls=%async_computation.1 | async-start | bytes 8388608 | tf_op jit(solution)/shard_map/all_to_all | solution.py:115
  327.4 0.2 reshape.197
  327.5 0.2 reduce_sum.61
  327.8 0.1 broadcast_bitcast_fusion
  327.9 0.1 copy.50
  328.0 0.1 broadcast_bitcast_fusion.1
  328.0 0.0 copy-done.2
  328.1 0.2 copy.51
  328.3 0.0 copy-done.3
  328.3 0.0 copy-done.6
  328.3 0.1 copy.57
  328.5 27.2 %all-gather.4.cloned.1.call-done = bf16[1536,2048]{1,0:T(8,128)(2,1)} async-done(((bf16[384,2048]{1,0:T(8,128)(2,1)}), bf16[1536,2048]{1,0:T(8,128)(2,1)}) %all-gather.4.cloned.1.call-update) | async-done | bytes 6291472 | tf_op jit(solution)/shard_map/all_gather | solution.py:88
  355.8 11.1 %convolution_convert_fusion = bf16[1536,1024]{1,0:T(8,128)(2,1)} fusion(bf16[1536,2048]{1,0:T(8,128)(2,1)} %all-gather.4.cloned.1.call-done, bf16[2048,1024]{1,0:T(8,128)(2,1)} %param.19), kind=kOutput, calls=%fused_computation.42 | convolution fusion | flops 6444023808 | bytes 13631488 | tf_op jit(solution)/shard_map/dot_general | solution.py:87
  366.9 54.2 %all-to-all-done.1 = bf16[4,4,128,1024]{3,0,1,2:T(4,128)(2,1)} async-done(((bf16[4,4,128,1024]{3,0,1,2:T(4,128)(2,1)}), bf16[4,4,128,1024]{3,0,1,2:T(4,128)(2,1)}, u32[]{:S(2)}, u32[]{:S(2)}) %all-to-all-start.1) | async-done | bytes 4194336 | tf_op jit(solution)/shard_map/all_to_all | solution.py:115
  421.1 6.4 %copy.55 = bf16[4,4,8,16,1024]{4,3,1,2,0:T(8,128)(2,1)} copy(bf16[4,4,8,16,1024]{4,0,1,3,2:T(4,128)(2,1)} %bitcast.56) | data formatting | bytes 8388608 | tf_op jit(solution)/shard_map/all_to_all | solution.py:115
  427.5 7.7 %gather_fusion = bf16[1024,1024]{1,0:T(8,128)(2,1)S(1)} fusion(bf16[2048,1024]{1,0:T(8,128)(2,1)} %bitcast.131, s32[1024]{0:T(1024)S(1)} %broadcast_clamp_fusion), kind=kCustom, calls=%fused_computation | custom fusion | bytes 4198400 | tf_op jit(solution)/shard_map/jit(_take)/gather | solution.py:121
  435.2 2.2 gather.15
  437.5 11.0 %multiply_reduce_fusion = bf16[512,1024]{1,0:T(8,128)(2,1)} fusion(bf16[512,2,1024]{2,1,0:T(2,128)(2,1)} %gather.15, pred[512,2]{1,0:T(8,128)(4,1)S(1)} %copy.51, f32[512,2]{1,0:T(8,128)S(1)} %copy.57), kind=kLoop, calls=%fused_computation.38 | loop fusion | flops 3670016 | bytes 3150848 | tf_op jit(solution)/shard_map/reduce_sum | solution.py:125
  (25 shorter events, 0.2 us)
Async XLA Ops:
  7.2 236.3 %all-gather.6.cloned.1.call-start = ((), (), s32[]{:S(2)}) async-start(), calls=%async_computation.3 | async-start | bytes 20971520 | tf_op jit(solution)/shard_map/all_gather | solution.py:101
  138.4 168.8 %all-gather.8.cloned.1.call-start = ((), (), s32[]{:S(2)}) async-start(), calls=%async_computation.4 | async-start | bytes 5242880 | tf_op jit(solution)/shard_map/all_gather | solution.py:111
  257.5 14.7 %copy-start = (bf16[384,2048]{1,0:T(8,128)(2,1)S(1)}, bf16[384,2048]{1,0:T(8,128)(2,1)}, u32[]{:S(2)}) copy-start(bf16[384,2048]{1,0:T(8,128)(2,1)} %param.15) | copy-start | bytes 4718596
  272.0 4.8 %copy-start.1 = (f32[31,2048]{1,0:T(8,128)S(1)}, f32[31,2048]{1,0:T(8,128)}, u32[]{:S(2)}) copy-start(f32[31,2048]{1,0:T(8,128)} %param.16) | copy-start | bytes 761860
  272.1 83.7 %all-gather.4.cloned.1.call-start = ((), (), s32[]{:S(2)}) async-start(), calls=%async_computation.2 | async-start | bytes 7864320 | tf_op jit(solution)/shard_map/all_gather | solution.py:88
  274.5 3.1 collective-permute-start
  277.6 14.8 %copy-start.4 = (f32[2048]{0:T(1024)S(1)}, f32[2048]{0:T(1024)}, u32[]{:S(2)}) copy-start(f32[2048]{0:T(1024)} %param.18) | copy-start | bytes 24580
  277.6 14.8 %copy-start.5 = (f32[2048]{0:T(1024)S(1)}, f32[2048]{0:T(1024)}, u32[]{:S(2)}) copy-start(f32[2048]{0:T(1024)} %param.17) | copy-start | bytes 24580
  321.7 6.3 %copy-start.2 = (s32[512,2]{0,1:T(2,128)S(1)}, s32[512,2]{0,1:T(2,128)}, u32[]{:S(2)}) copy-start(s32[512,2]{0,1:T(2,128)} %param.22) | copy-start | bytes 12292
  321.7 6.6 %copy-start.3 = (f32[512,2]{0,1:T(2,128)S(1)}, f32[512,2]{0,1:T(2,128)}, u32[]{:S(2)}) copy-start(f32[512,2]{0,1:T(2,128)} %param.24) | copy-start | bytes 12292
  321.7 6.6 %copy-start.6 = (f32[512]{0:T(512)S(1)}, f32[512]{0:T(512)}, u32[]{:S(2)}) copy-start(f32[512]{0:T(512)} %param.23) | copy-start | bytes 6148
  321.7 99.3 %all-to-all-start.1 = ((bf16[4,4,128,1024]{3,0,1,2:T(4,128)(2,1)}), bf16[4,4,128,1024]{3,0,1,2:T(4,128)(2,1)}, u32[]{:S(2)}, u32[]{:S(2)}) async-start(bf16[4,4,128,1024]{3,0,1,2:T(4,128)(2,1)} %copy.54), calls=%async_computation.1 | async-start | bytes 8388608 | tf_op jit(solution)/shard_map/all_to_all | solution.py:115
Sparse Core Ops, SparseCore 0:
  138.6 104.8 all-gather.5
  272.2 34.9 all-gather.7
  309.4 46.3 all-gather.3
where the time goes:
time: 456 us; the launch traced here: 455 us
  waiting for transfers between devices  199 us (44%)
  blocking collectives  100 us (22%)
  matrix products  48.8 us (11%)
  local copies, waits for them, and re-layouts  45.5 us (10%)
  other arithmetic  38.8 us (9%)
  between operations  14 us (3%)
  starting transfers between devices  8.33 us (2%)
    all_gather x1, waiting for transfers between devices, on_device(): hidden_arrived = lax.all_gather(arrived, 'tp', axis=0, tiled=True)  105 us
    all_to_all x1, blocking collectives, on_device(): lax.all_to_all(outgoing, 'ep', split_axis=1, concat_axis=2, tiled=True)  100 us
    all_to_all x1, waiting for transfers between devices, on_device(): lax.all_to_all(summed.astype(jnp.bfloat16), 'ep', split_axis=2, concat_ax...  54.2 us
    all_gather x1, waiting for transfers between devices, on_device(): lax.all_gather(activated, 'tp', axis=0, tiled=True)  27.2 us
    gather x2, local copies, waits for them, and re-layouts, take_rows(): return jnp.take(normed, jnp.maximum(source, 0), axis=0)  17.4 us
    dot_general x1, matrix products, on_device(): jnp.einsum('qecd,edh->qech', hidden_arrived, gate_weight, preferred_eleme...  14.6 us
    reduce_sum x1, other arithmetic, on_device(): center = mixed_conv - jnp.mean(mixed_conv, axis=-1, keepdims=True)  14.3 us
    dot_general x1, matrix products, on_device(): jnp.einsum('qecd,edh->qech', hidden_arrived, up_weight, preferred_element...  14 us
  transfers between devices with their start and end apart: 5, of which 5 were waited for; matrix products, arithmetic and copies ran while one was open for 10% of the time, Pallas kernels for 0%

commit v1 on v0

--- a/solution.py
+++ b/solution.py
@@ -8,6 +8,17 @@
 MOE_DEV = 128
 CAP = 16
 epsilon = 1e-06
+
+
+def gather_by_hops(x, axis, dim):
+    size = lax.axis_size(axis)
+    route = [(i, (i + 1) % size) for i in range(size)]
+    parts = [x]
+    for stride in range(1, size):
+        parts = [lax.ppermute(parts[0], axis, route), *parts]
+    whole = jnp.concatenate(parts, axis=dim)
+    offset = (lax.axis_index(axis) + 1) * parts[-1].shape[dim]
+    return jnp.roll(whole, offset, axis=dim)
 
 
 def passed_along(value, axis, steps):
@@ -98,7 +109,7 @@
     own_positions = lax.dynamic_slice_in_dim(positions, own_quarter, 1, 0)
     outgoing = fill_slots(normed, own_experts, own_positions)
     arrived = lax.all_to_all(outgoing, "ep", split_axis=1, concat_axis=2, tiled=True)
-    hidden_arrived = lax.all_gather(arrived, "tp", axis=0, tiled=True)
+    hidden_arrived = gather_by_hops(arrived, "tp", 0)
     gate_part = jnp.einsum(
         "qecd,edh->qech", hidden_arrived, gate_weight, preferred_element_type=jnp.float32
     )

time: 456 us -> 529 us (1.16)
  waiting for transfers between devices: 199 us -> 238 us
  local copies, waits for them, and re-layouts: 45.5 us -> 77 us
    ppermute x0 -> x3, waiting for transfers between devices: none -> 144 us  [gather_by_hops(): parts = [lax.ppermute(parts[0], axis, route), *parts]]
    all_gather x1 -> x0, waiting for transfers between devices: 105 us -> none  [on_device(): hidden_arrived = lax.all_gather(arrived, 'tp', axis=0, tiled=True)]
    unnamed x18 -> x33, local copies, waits for them, and re-layouts: 0.94 us -> 31.9 us
  transfers between devices with their start and end apart: 5 -> 7, of which waited for: 5 -> 7; matrix products, arithmetic and copies ran while one was open for 10% -> 9% of each run, Pallas kernels for 0% -> 0%
where the time goes in v1:
time: 529 us; the launch traced here: 523 us
  waiting for transfers between devices  238 us (45%)
  blocking collectives  100 us (19%)
  local copies, waits for them, and re-layouts  77 us (15%)
  matrix products  46.3 us (9%)
  other arithmetic  38.8 us (7%)
  between operations  14.6 us (3%)
  starting transfers between devices  7.85 us (1%)
    ppermute x3, waiting for transfers between devices, gather_by_hops(): parts = [lax.ppermute(parts[0], axis, route), *parts]  144 us
    all_to_all x1, blocking collectives, on_device(): lax.all_to_all(outgoing, 'ep', split_axis=1, concat_axis=2, tiled=True)  100 us
    all_to_all x1, waiting for transfers between devices, on_device(): lax.all_to_all(summed.astype(jnp.bfloat16), 'ep', split_axis=2, concat_ax...  54.4 us
    unnamed x33, local copies, waits for them, and re-layouts  31.9 us
    all_gather x1, waiting for transfers between devices, on_device(): lax.all_gather(activated, 'tp', axis=0, tiled=True)  27 us
    gather x2, local copies, waits for them, and re-layouts, take_rows(): return jnp.take(normed, jnp.maximum(source, 0), axis=0)  17.4 us
    reduce_sum x1, other arithmetic, on_device(): center = mixed_conv - jnp.mean(mixed_conv, axis=-1, keepdims=True)  14.3 us
    dot_general x1, matrix products, on_device(): jnp.einsum('qecd,edh->qech', hidden_arrived, gate_weight, preferred_eleme...  14 us
  transfers between devices with their start and end apart: 7, of which 7 were waited for; matrix products, arithmetic and copies ran while one was open for 9% of the time, Pallas kernels for 0%

profile of v1, /device:TPU:0, one launch (start us, length us, event | category | flops | bytes accessed | tf_op | source)
XLA Modules:
  0.0 523.3 jit_solution(12568206466390464977)
XLA Ops:
  7.2 0.0 all-gather.5.cloned.1.call-start
  7.2 0.8 copy.45
  8.0 0.2 eq.32
  8.2 0.2 eq.28
  8.4 2.3 reduce-window.6
  10.8 0.1 slice.321
  10.9 0.1 copy.47
  11.0 0.1 fusion.53
  11.2 1.4 scatter_custom_fusion
  12.6 1.5 fusion.10
  14.2 0.1 broadcast_in_dim.62
  14.3 0.1 broadcast_in_dim.64
  14.3 1.6 fusion.50
  15.9 17.4 %gather_fusion.1 = bf16[512,4096]{1,0:T(8,128)(2,1)} fusion(bf16[1,128,4096]{2,1,0:T(8,128)(2,1)S(1)} %fusion.50, s32[512]{0:T(512)S(1)} %bitcast.133), kind=kCustom, calls=%fused_computation.1 | custom fusion | bytes 8392704 | tf_op jit(solution)/shard_map/vmap(jit(_take))/gather | solution.py:50
  33.3 2.6 select_select_fusion
  35.9 100.3 %all_to_all.33 = bf16[1,32,16,4096]{3,2,0,1:T(8,128)(2,1)S(1)} all-to-all(bf16[1,32,16,4096]{3,2,0,1:T(8,128)(2,1)S(1)} %select_select_fusion), channel_id=1, replica_groups=mesh['ep'=8,'tp'=4] {'ep'}, dimensions={1} | all-to-all | bytes 8388608 | tf_op jit(solution)/shard_map/all_to_all | solution.py:111
  136.2 0.5 copy.53
  136.7 1.9 copy-done
  138.6 47.9 %collective-permute-done.1 = bf16[1,4,128,4096]{3,2,0,1:T(8,128)(2,1)S(1)} collective-permute-done((bf16[1,4,128,4096]{3,2,0,1:T(8,128)(2,1)S(1)}, bf16[1,4,128,4096]{3,2,0,1:T(8,128)(2,1)S(1)}, u32[]{:S(2)}, u32[]{:S(2)}) %collective-permute-start.1) | collective-permute-done | bytes 4194336 | tf_op jit(solution)/shard_map/ppermute | solution.py:18
  186.6 1.9 copy-done.2
  188.5 0.0 collective-permute-start.2
  188.5 48.0 %collective-permute-done.2 = bf16[1,4,128,4096]{3,2,0,1:T(8,128)(2,1)} collective-permute-done((bf16[1,4,128,4096]{3,2,0,1:T(8,128)(2,1)S(1)}, bf16[1,4,128,4096]{3,2,0,1:T(8,128)(2,1)}, u32[]{:S(2)}, u32[]{:S(2)}) %collective-permute-start.2) | collective-permute-done | bytes 4194336 | tf_op jit(solution)/shard_map/ppermute | solution.py:18
  236.5 0.5 collective-permute-start.3
  237.0 48.2 %collective-permute-done.3 = bf16[1,4,128,4096]{3,2,0,1:T(8,128)(2,1)} collective-permute-done((bf16[1,4,128,4096]{3,2,0,1:T(8,128)(2,1)}, bf16[1,4,128,4096]{3,2,0,1:T(8,128)(2,1)}, u32[]{:S(2)}, u32[]{:S(2)}) %collective-permute-start.3) | collective-permute-done | bytes 4194336 | tf_op jit(solution)/shard_map/ppermute | solution.py:18
  285.2 4.7 constant_dynamic-update-slice_fusion.7
  290.0 4.8 constant_dynamic-update-slice_fusion.6
  294.8 2.4 constant_dynamic-update-slice_fusion.5
  297.2 1.3 copy-done.1
  298.5 2.3 constant_dynamic-update-slice_fusion.4
  300.8 4.7 constant_dynamic-update-slice_fusion.3
  305.5 4.7 constant_dynamic-update-slice_fusion.2
  310.1 2.2 constant_dynamic-update-slice_fusion.1
  312.4 2.3 constant_dynamic-update-slice_fusion
  314.7 14.0 %fusion.2 = f32[4,4,128,256]{3,2,1,0:T(8,128)} fusion(bf16[8,4,128,4096]{3,2,0,1:T(8,128)(2,1)} %constant_dynamic-update-slice_fusion, s32[]{:T(128)S(6)} %select_n.94, bf16[4,4096,256]{2,1,0:T(8,128)(2,1)} %param.25), kind=kOutput, calls=%fused_computation.34 | convolution fusion | flops 4294967296 | bytes 27262980 | tf_op jit(solution)/shard_map/qecd,edh->qech/dot_general | solution.py:113
  328.7 12.0 %fusion.13 = bf16[4,4,128,256]{3,2,0,1:T(8,128)(2,1)} fusion(f32[4,4,128,256]{3,2,1,0:T(8,128)} %fusion.2, bf16[4,4096,256]{2,1,0:T(8,128)(2,1)} %param.26, bf16[8,4,128,4096]{3,2,0,1:T(8,128)(2,1)} %constant_dynamic-update-slice_fusion, s32[]{:T(128)S(6)} %select_n.94), kind=kOutput, calls=%fused_computation.55 | convolution fusion | flops 4298113024 | bytes 28311556 | tf_op jit(solution)/shard_map/qecd,edh->qech/dot_general | solution.py:116
  340.7 0.0 all-gather.5.cloned.1.call-update
  340.7 0.0 all-gather.3.cloned.1.call-start
  340.8 2.3 multiply_convert_fusion.1
  343.1 1.5 collective-permute-start
  344.6 0.1 fusion.66
  344.7 0.1 fusion.67
  344.8 0.6 collective-permute-done
  345.4 14.3 %fusion.65 = (f32[384]{0:T(512)S(1)}, f32[384,2048]{1,0:T(8,128)S(1)}) fusion(bf16[384,2048]{1,0:T(8,128)(2,1)S(1)} %multiply_convert_fusion.1, bf16[30,2048]{1,0:T(8,128)(2,1)S(1)} %collective-permute-done, f32[2048]{0:T(1024)S(1)} %bitcast.166, f32[2048]{0:T(1024)S(1)} %bitcast.167, f32[2048]{0:T(1024)S(1)} %bitcast.138, f32[2048]{0:T(1024)S(1)} %bitcast.139, ...), kind=kLoop, calls=%fused_computation.148 | loop fusion | flops 143916672 | bytes 5096960 | tf_op jit(solution)/shard_map/reduce_sum | solution.py:93
  359.7 0.5 multiply_reduce_fusion.1
  360.2 2.4 multiply_convert_fusion
  362.6 0.0 all-gather.3.cloned.1.call-update
  362.6 12.3 %all-gather.5.cloned.1.call-done = bf16[4,4,128,1024]{3,2,0,1:T(8,128)(2,1)} async-done(((bf16[4,4,128,256]{3,2,0,1:T(8,128)(2,1)}), bf16[4,4,128,1024]{3,2,0,1:T(8,128)(2,1)}) %all-gather.5.cloned.1.call-update) | async-done | bytes 4194320 | tf_op jit(solution)/shard_map/all_gather | solution.py:122
  374.9 9.2 %convert_bitcast_fusion = bf16[4,4,128,1024]{3,2,0,1:T(8,128)(2,1)S(1)} fusion(bf16[4,4,128,1024]{3,2,0,1:T(8,128)(2,1)} %all-gather.5.cloned.1.call-done, bf16[4,1024,1024]{2,1,0:T(8,128)(2,1)} %param.27), kind=kOutput, calls=%fused_computation.41 | convolution fusion | flops 4297064448 | bytes 16777216 | tf_op jit(solution)/shard_map/qech,ehd->qecd/dot_general | solution.py:120
  384.1 5.3 %copy.54 = bf16[4,4,128,1024]{3,0,1,2:T(4,128)(2,1)} copy(bf16[4,4,128,1024]{3,2,0,1:T(8,128)(2,1)S(1)} %convert_bitcast_fusion) | data formatting | bytes 8388608 | tf_op jit(solution)/shard_map/convert_element_type | solution.py:127
  389.4 5.8 %all-to-all-start.1 = ((bf16[4,4,128,1024]{3,0,1,2:T(4,128)(2,1)}), bf16[4,4,128,1024]{3,0,1,2:T(4,128)(2,1)}, u32[]{:S(2)}, u32[]{:S(2)}) async-start(bf16[4,4,128,1024]{3,0,1,2:T(4,128)(2,1)} %copy.54), calls=%async_computation.1 | async-start | bytes 8388608 | tf_op jit(solution)/shard_map/all_to_all | solution.py:126
  395.2 0.2 reshape.197
  395.4 0.2 reduce_sum.61
  395.6 0.1 broadcast_bitcast_fusion
  395.7 0.1 copy.50
  395.8 0.1 broadcast_bitcast_fusion.1
  395.9 0.2 copy.51
  396.2 0.1 copy.57
  396.4 27.0 %all-gather.3.cloned.1.call-done = bf16[1536,2048]{1,0:T(8,128)(2,1)} async-done(((bf16[384,2048]{1,0:T(8,128)(2,1)}), bf16[1536,2048]{1,0:T(8,128)(2,1)}) %all-gather.3.cloned.1.call-update) | async-done | bytes 6291472 | tf_op jit(solution)/shard_map/all_gather | solution.py:99
  423.4 11.1 %convolution_convert_fusion = bf16[1536,1024]{1,0:T(8,128)(2,1)} fusion(bf16[1536,2048]{1,0:T(8,128)(2,1)} %all-gather.3.cloned.1.call-done, bf16[2048,1024]{1,0:T(8,128)(2,1)} %param.19), kind=kOutput, calls=%fused_computation.44 | convolution fusion | flops 6444023808 | bytes 13631488 | tf_op jit(solution)/shard_map/dot_general | solution.py:98
  434.5 54.4 %all-to-all-done.1 = bf16[4,4,128,1024]{3,0,1,2:T(4,128)(2,1)} async-done(((bf16[4,4,128,1024]{3,0,1,2:T(4,128)(2,1)}), bf16[4,4,128,1024]{3,0,1,2:T(4,128)(2,1)}, u32[]{:S(2)}, u32[]{:S(2)}) %all-to-all-start.1) | async-done | bytes 4194336 | tf_op jit(solution)/shard_map/all_to_all | solution.py:126
  488.9 6.4 %copy.55 = bf16[4,4,8,16,1024]{4,3,1,2,0:T(8,128)(2,1)} copy(bf16[4,4,8,16,1024]{4,0,1,3,2:T(4,128)(2,1)} %bitcast.56) | data formatting | bytes 8388608 | tf_op jit(solution)/shard_map/all_to_all | solution.py:126
  495.3 7.7 %gather_fusion = bf16[1024,1024]{1,0:T(8,128)(2,1)S(1)} fusion(bf16[2048,1024]{1,0:T(8,128)(2,1)} %bitcast.129, s32[1024]{0:T(1024)S(1)} %broadcast_clamp_fusion), kind=kCustom, calls=%fused_computation | custom fusion | bytes 4198400 | tf_op jit(solution)/shard_map/jit(_take)/gather | solution.py:132
  503.0 2.2 gather.15
  505.2 11.0 %multiply_reduce_fusion = bf16[512,1024]{1,0:T(8,128)(2,1)} fusion(bf16[512,2,1024]{2,1,0:T(2,128)(2,1)} %gather.15, pred[512,2]{1,0:T(8,128)(4,1)S(1)} %copy.51, f32[512,2]{1,0:T(8,128)S(1)} %copy.57), kind=kLoop, calls=%fused_computation.40 | loop fusion | flops 3670016 | bytes 3150848 | tf_op jit(solution)/shard_map/reduce_sum | solution.py:136
  (44 shorter events, 0.3 us)
Async XLA Ops:
  7.2 367.7 %all-gather.5.cloned.1.call-start = ((), (), s32[]{:S(2)}) async-start(), calls=%async_computation.3 | async-start | bytes 5242880 | tf_op jit(solution)/shard_map/all_gather | solution.py:122
  136.7 1.9 copy-start
  138.6 47.9 %collective-permute-start.1 = (bf16[1,4,128,4096]{3,2,0,1:T(8,128)(2,1)S(1)}, bf16[1,4,128,4096]{3,2,0,1:T(8,128)(2,1)S(1)}, u32[]{:S(2)}, u32[]{:S(2)}) collective-permute-start(bf16[1,4,128,4096]{3,2,0,1:T(8,128)(2,1)S(1)} %bitcast.130), channel_id=1, source_target_pairs={{0,1},{1,2},{2,3},{3,0},{4,5},{5,6},{6,7},{7,4},{8,9},{9,10},{10,1... | collective-permute-start | bytes 12582920 | tf_op jit(solution)/shard_map/ppermute | solution.py:18
  186.6 1.9 copy-start.2
  188.5 48.0 %collective-permute-start.2 = (bf16[1,4,128,4096]{3,2,0,1:T(8,128)(2,1)S(1)}, bf16[1,4,128,4096]{3,2,0,1:T(8,128)(2,1)}, u32[]{:S(2)}, u32[]{:S(2)}) collective-permute-start(bf16[1,4,128,4096]{3,2,0,1:T(8,128)(2,1)S(1)} %collective-permute-done.1), channel_id=1, source_target_pairs={{0,1},{1,2},{2,3},{3,0},{4,5},{5,6},{6,7},{7,4},{8,9},{9,10},{10,1... | collective-permute-start | bytes 12582920 | tf_op jit(solution)/shard_map/ppermute | solution.py:18
  236.5 48.7 %collective-permute-start.3 = (bf16[1,4,128,4096]{3,2,0,1:T(8,128)(2,1)}, bf16[1,4,128,4096]{3,2,0,1:T(8,128)(2,1)}, u32[]{:S(2)}, u32[]{:S(2)}) collective-permute-start(bf16[1,4,128,4096]{3,2,0,1:T(8,128)(2,1)} %collective-permute-done.2), channel_id=1, source_target_pairs={{0,1},{1,2},{2,3},{3,0},{4,5},{5,6},{6,7},{7,4},{8,9},{9,10},{10,1... | collective-permute-start | bytes 12582920 | tf_op jit(solution)/shard_map/ppermute | solution.py:18
  290.0 4.8 copy-start.3
  294.8 3.7 copy-start.1
  328.7 12.1 %copy-start.4 = (bf16[384,2048]{1,0:T(8,128)(2,1)S(1)}, bf16[384,2048]{1,0:T(8,128)(2,1)}, u32[]{:S(2)}) copy-start(bf16[384,2048]{1,0:T(8,128)(2,1)} %param.15) | copy-start | bytes 4718596
  340.7 3.9 copy-start.5
  340.7 82.7 %all-gather.3.cloned.1.call-start = ((), (), s32[]{:S(2)}) async-start(), calls=%async_computation.2 | async-start | bytes 7864320 | tf_op jit(solution)/shard_map/all_gather | solution.py:99
  343.1 2.3 collective-permute-start
  345.4 14.8 %copy-start.8 = (f32[2048]{0:T(1024)S(1)}, f32[2048]{0:T(1024)}, u32[]{:S(2)}) copy-start(f32[2048]{0:T(1024)} %param.18) | copy-start | bytes 24580
  345.4 14.8 %copy-start.9 = (f32[2048]{0:T(1024)S(1)}, f32[2048]{0:T(1024)}, u32[]{:S(2)}) copy-start(f32[2048]{0:T(1024)} %param.17) | copy-start | bytes 24580
  389.4 6.5 %copy-start.6 = (s32[512,2]{0,1:T(2,128)S(1)}, s32[512,2]{0,1:T(2,128)}, u32[]{:S(2)}) copy-start(s32[512,2]{0,1:T(2,128)} %param.22) | copy-start | bytes 12292
  389.4 6.8 %copy-start.7 = (f32[512,2]{0,1:T(2,128)S(1)}, f32[512,2]{0,1:T(2,128)}, u32[]{:S(2)}) copy-start(f32[512,2]{0,1:T(2,128)} %param.24) | copy-start | bytes 12292
  389.4 6.8 %copy-start.10 = (f32[512]{0:T(512)S(1)}, f32[512]{0:T(512)}, u32[]{:S(2)}) copy-start(f32[512]{0:T(512)} %param.23) | copy-start | bytes 6148
  389.4 99.5 %all-to-all-start.1 = ((bf16[4,4,128,1024]{3,0,1,2:T(4,128)(2,1)}), bf16[4,4,128,1024]{3,0,1,2:T(4,128)(2,1)}, u32[]{:S(2)}, u32[]{:S(2)}) async-start(bf16[4,4,128,1024]{3,0,1,2:T(4,128)(2,1)} %copy.54), calls=%async_computation.1 | async-start | bytes 8388608 | tf_op jit(solution)/shard_map/all_to_all | solution.py:126
Sparse Core Ops, SparseCore 0:
  340.8 34.0 all-gather.4
  377.0 46.2 all-gather.2
